TPU v7x, 256 devices: a whole 4x4x8 slice. The times are simulated.
256 devices in a mesh: ep: 32 (over z, x), tp: 8 (over y, core).
Axes of the slice: x: 4, y: 4, z: 8, core: 2. Of those that a mesh axis runs over, the one named last changes fastest.
Arguments:
- resid: bfloat16 [1024, 2048], P('ep'), may hold values from -6 to 6
- norm_gain: bfloat16 [2048], replicated, may hold values from 0.099609375 to 1.8984375
- w_query: bfloat16 [2048, 1024], P(None, 'tp'), may hold values from -0.125 to 0.125
- w_key: bfloat16 [2048, 1024], P(None, 'tp'), may hold values from -0.125 to 0.125
- w_value: bfloat16 [2048, 1024], P(None, 'tp'), may hold values from -0.125 to 0.125
- w_gate: bfloat16 [2048, 1024], P(None, 'tp'), may hold values from -0.125 to 0.125
- head_gain: bfloat16 [1024], P('tp'), may hold values from 0.099609375 to 1.8984375
- w_output: bfloat16 [1024, 2048], P('tp'), may hold values from -0.1875 to 0.1875
- state: float32 [1024, 8, 128, 128], P('ep', 'tp'), may hold values from -0.6 to 0.6
- positions: int32 [1024], P('ep'), may hold values from 1024 to 8191
- ffn_gain: bfloat16 [2048], replicated, may hold values from 0.099609375 to 1.8984375
- w_mix: bfloat16 [2048], replicated, may hold values from -0.125 to 0.125
- dense_gate: bfloat16 [2048, 5632], P('tp', 'ep'), may hold values from -0.125 to 0.125
- dense_up: bfloat16 [2048, 5632], P('tp', 'ep'), may hold values from -0.125 to 0.125
- dense_down: bfloat16 [5632, 2048], P('ep', 'tp'), may hold values from -0.15625 to 0.15625
- routes: int32 [1024, 2], P('ep'), may hold values from 0 to 31, all different within a row; in each aligned block of 32 rows (0 to 31, 32 to 63, ...) at most 4 rows name the same one
- route_weight: bfloat16 [1024, 2], P('ep'), may hold values from 0.19921875 to 1
- expert_gate: bfloat16 [32, 2048, 4096], P('ep', None, 'tp'), may hold values from -0.125 to 0.125
- expert_up: bfloat16 [32, 2048, 4096], P('ep', None, 'tp'), may hold values from -0.125 to 0.125
- expert_down: bfloat16 [32, 4096, 2048], P('ep', 'tp'), may hold values from -0.09375 to 0.09375
Outputs:
- final: bfloat16 [1024, 2048], P('ep', 'tp')
- new_state: float32 [1024, 8, 128, 128], P('ep', 'tp')
Inputs may be any that keep to these rules, and one draw needn't show every extreme that they name: `routes`: each row names 2 different experts; in the rows of one index of ep no expert is named by more than 4 rows, a bound that some block reaches; every expert is named by some row.
All inputs are finite; a program needn't handle non-finite values.
Results may differ from a plain program's by a relative error of at most 0.018.
Values may be sent and summed in bfloat16 or wider, within the bound.
No kernel may reach another device: no remote copies, remote signals or barrier semaphores. Data moves between devices by JAX's collectives and lax.ppermute only.
A program may use at most 64 MiB of HBM per device.

v0:
```python
import jax
import jax.numpy as jnp
from jax import lax
from jax.sharding import PartitionSpec as P

EPSILON = 1e-06
THETA = 10000.0


def split_up(value, dim, length):
    before, after = (value.shape[:dim], value.shape[dim + 1 :])
    return jnp.moveaxis(value.reshape(*before, length, -1, *after), dim, 0)


def sent_and_summed(value, axis, dim):
    tiles = split_up(value, dim, lax.axis_size(axis))
    arrived = lax.all_to_all(tiles, axis, split_axis=0, concat_axis=0, tiled=True)
    return arrived.astype(jnp.float32).sum(axis=0)


def copy_for_each(value, axis):
    copies = jnp.broadcast_to(value, (lax.axis_size(axis), *value.shape))
    return lax.all_to_all(copies, axis, split_axis=0, concat_axis=0, tiled=True)


def of_everyone(value, axis):
    everything = copy_for_each(value, axis)
    return jnp.sum(everything.astype(jnp.float32), axis=0)


def in_order(tiles, dim):
    dims = list(tiles.shape[1:])
    dims[dim] *= tiles.shape[0]
    return jnp.moveaxis(tiles, 0, dim).reshape(dims)


def gather_directly(value, axis, dim):
    tiles = copy_for_each(value, axis)
    return in_order(tiles, dim)


def packed_total(arrays, axis):
    flat, at, outs = (jnp.concatenate([a.reshape(-1) for a in arrays]), 0, [])
    running = lax.psum(flat, axis)
    for a in arrays:
        outs.append(running[at : at + a.size].reshape(a.shape))
        at += a.size
    return tuple(outs)


def rms_norm(inputs, scaling):
    square = jnp.mean(inputs * inputs, axis=-1, keepdims=True)
    return inputs * lax.rsqrt(square + EPSILON) * scaling.astype(jnp.float32)


def rotate(inputs, places):
    halfway = inputs.shape[-1] // 2
    inverse = THETA ** (-jnp.arange(halfway, dtype=jnp.float32) / halfway)
    angles = places.astype(jnp.float32)[:, None] * inverse[None, :]
    cosine = jnp.cos(angles)[:, None, :]
    sine_of = jnp.sin(angles)[:, None, :]
    former = inputs[..., :halfway]
    latter = inputs[..., halfway:]
    return jnp.concatenate(
        [former * cosine - latter * sine_of, former * sine_of + latter * cosine], axis=-1
    )


def retain(queries, keys_in, values_in, gating, memory, places, head_first, head_gain):
    seqs_here = queries.shape[0]
    heads_here = memory.shape[1]
    head_size = memory.shape[2]
    head_shape = (seqs_here, heads_here, head_size)
    query_rot = rotate(queries.astype(jnp.float32).reshape(head_shape), places)
    key_rot = rotate(keys_in.astype(jnp.float32).reshape(head_shape), places) * head_size ** (-0.5)
    value_heads = values_in.astype(jnp.float32).reshape(head_shape)
    head_index = head_first + jnp.arange(heads_here, dtype=jnp.float32)
    decays = 1.0 - jnp.exp2(-1.0 - 1.5 * head_index)
    within = jnp.sum(query_rot * key_rot, axis=-1, keepdims=True) * value_heads
    carried = jnp.einsum("shd,shde->she", query_rot, memory) * decays[None, :, None]
    mixture = within + carried
    new_memory = (
        decays[None, :, None, None] * memory + key_rot[:, :, :, None] * value_heads[:, :, None, :]
    )
    centre = jnp.mean(mixture, axis=-1, keepdims=True)
    spread = jnp.mean(jnp.square(mixture - centre), axis=-1, keepdims=True)
    normed = ((mixture - centre) * lax.rsqrt(spread + EPSILON)).reshape(
        seqs_here, heads_here * head_size
    )
    normed = normed * head_gain.astype(jnp.float32)
    output = (jax.nn.silu(gating.astype(jnp.float32)) * normed).astype(jnp.bfloat16)
    return (output, new_memory)


def expert_hidden(chosen, gate_weight, up_weight):
    gate_value = jnp.dot(chosen, gate_weight, preferred_element_type=jnp.float32)
    up_value = jnp.dot(chosen, up_weight, preferred_element_type=jnp.float32)
    return (jax.nn.silu(gate_value) * up_value).astype(jnp.bfloat16)


def padded_experts(
    normed_mid, routes, route_weight, expert_gate, expert_up, expert_down, capacity, experts_all
):
    seq_dev, model_width = normed_mid.shape
    top_count = routes.shape[1]
    flat_ids = routes.reshape(-1)
    expert_ids = jnp.arange(experts_all, dtype=jnp.int32)
    onehot = (flat_ids[:, None] == expert_ids[None, :]).astype(jnp.int32)
    ranks = jnp.sum((jnp.cumsum(onehot, axis=0) - 1) * onehot, axis=1)
    slot_ids = flat_ids * capacity + ranks
    slot_range = jnp.arange(experts_all * capacity, dtype=jnp.int32)
    dispatch = (slot_range[:, None] == slot_ids[None, :]).astype(jnp.bfloat16)
    repeated = jnp.repeat(normed_mid, top_count, axis=0)
    outgoing = jnp.dot(dispatch, repeated, preferred_element_type=jnp.float32).astype(jnp.bfloat16)
    outgoing = outgoing.reshape(experts_all, capacity, model_width)
    arrived = lax.all_to_all(outgoing, "ep", split_axis=0, concat_axis=0, tiled=True)
    sources = arrived.shape[0]
    items = arrived.shape[1]
    hidden_e = expert_hidden(
        arrived.reshape(sources * items, model_width), expert_gate[0], expert_up[0]
    )
    partial_value = jnp.dot(hidden_e, expert_down[0], preferred_element_type=jnp.float32)
    summed = sent_and_summed(partial_value.astype(jnp.bfloat16), "tp", 1).astype(jnp.bfloat16)
    returned = lax.all_to_all(
        summed.reshape(sources, items, summed.shape[1]),
        "ep",
        split_axis=0,
        concat_axis=0,
        tiled=True,
    )
    flat_back = returned.reshape(experts_all * capacity, returned.shape[2])
    weighted = flat_back[slot_ids].astype(jnp.float32) * route_weight.reshape(-1)[:, None].astype(
        jnp.float32
    )
    return jnp.sum(weighted.reshape(seq_dev, top_count, weighted.shape[1]), axis=1)


def per_device(
    resid,
    norm_gain,
    w_query,
    w_key,
    w_value,
    w_gate,
    head_gain,
    w_output,
    state,
    positions,
    ffn_gain,
    w_mix,
    dense_gate,
    dense_up,
    dense_down,
    routes,
    route_weight,
    expert_gate,
    expert_up,
    expert_down,
):
    seq_dev = resid.shape[0]
    model_width = resid.shape[1]
    tp_count = lax.axis_size("tp")
    ep_count = lax.axis_size("ep")
    model_tp = model_width // tp_count
    tp_index = lax.axis_index("tp")
    normed_in = rms_norm(resid.astype(jnp.float32), norm_gain).astype(jnp.bfloat16)

    def project(weight):
        return jnp.dot(normed_in, weight, preferred_element_type=jnp.float32).astype(jnp.bfloat16)

    heads_here = state.shape[1]
    head_first = (tp_index * heads_here).astype(jnp.float32)
    retained, new_state = retain(
        project(w_query),
        project(w_key),
        project(w_value),
        project(w_gate),
        state,
        positions,
        head_first,
        head_gain,
    )
    partial_value = jnp.dot(retained, w_output, preferred_element_type=jnp.float32)
    attention = of_everyone(partial_value.astype(jnp.bfloat16), "tp").astype(jnp.float32)
    middle = resid.astype(jnp.float32) + attention
    normed_mid = rms_norm(middle, ffn_gain).astype(jnp.bfloat16)
    mixing = jax.nn.sigmoid(jnp.dot(normed_mid, w_mix[:, None], preferred_element_type=jnp.float32))

    def own_columns(matrix):
        return lax.dynamic_slice_in_dim(matrix, tp_index * model_tp, model_tp, 1)

    top_count = routes.shape[1]
    capacity = max(2, 2 * seq_dev * top_count // ep_count)
    dense_rows = gather_directly(own_columns(normed_mid), "ep", 0)
    moe_out = padded_experts(
        normed_mid, routes, route_weight, expert_gate, expert_up, expert_down, capacity, ep_count
    )
    gate_part = jnp.dot(dense_rows, dense_gate, preferred_element_type=jnp.float32)
    up_part = jnp.dot(dense_rows, dense_up, preferred_element_type=jnp.float32)
    gate_sum, up_sum = tuple(
        (
            part.astype(jnp.float32)
            for part in packed_total(
                (gate_part.astype(jnp.bfloat16), up_part.astype(jnp.bfloat16)), "tp"
            )
        )
    )
    dense_hidden = (jax.nn.silu(gate_sum) * up_sum).astype(jnp.bfloat16)
    dense_out = sent_and_summed(
        jnp.dot(dense_hidden, dense_down, preferred_element_type=jnp.float32).astype(jnp.bfloat16),
        "ep",
        0,
    )
    final = (own_columns(middle) + moe_out + mixing * dense_out).astype(jnp.bfloat16)
    return (final, new_state)


def solution(mesh):
    in_specs = (
        P("ep", None),
        P(),
        P(None, "tp"),
        P(None, "tp"),
        P(None, "tp"),
        P(None, "tp"),
        P("tp"),
        P("tp", None),
        P("ep", "tp", None, None),
        P("ep"),
        P(),
        P(),
        P("tp", "ep"),
        P("tp", "ep"),
        P("ep", "tp"),
        P("ep", None),
        P("ep", None),
        P("ep", None, "tp"),
        P("ep", None, "tp"),
        P("ep", "tp", None),
    )
    out_specs = (P("ep", "tp"), P("ep", "tp", None, None))
    return jax.shard_map(
        per_device, mesh=mesh, in_specs=in_specs, out_specs=out_specs, check_vma=False
    )
```

profile of v0, /device:TPU:24, one launch (start us, length us, event | category | flops | bytes accessed | tf_op | source)
XLA Modules:
  0.0 206.2 jit_solution(7254978397219586404)
XLA Ops:
  8.7 1.0 fusion.25
  10.5 1.4 fusion.18
  11.9 1.4 fusion.20
  13.6 2.0 fusion.66
  16.8 1.5 convolution_convert_fusion.2
  18.4 1.1 broadcast_in_dim.6
  19.5 5.4 %all-to-all-start = ((bf16[8,32,2048]{2,1,0:T(8,128)(2,1)}), bf16[8,32,2048]{2,1,0:T(8,128)(2,1)S(1)}, u32[]{:S(2)}, u32[]{:S(2)}) async-start(bf16[8,32,2048]{2,1,0:T(8,128)(2,1)} %broadcast_in_dim.6), calls=%async_computation | async-start | bytes 2097152 | tf_op jit(solution)/shard_map/all_to_all | solution.py:23
  25.0 13.7 %all-to-all-done = bf16[8,32,2048]{2,1,0:T(8,128)(2,1)S(1)} async-done(((bf16[8,32,2048]{2,1,0:T(8,128)(2,1)}), bf16[8,32,2048]{2,1,0:T(8,128)(2,1)S(1)}, u32[]{:S(2)}, u32[]{:S(2)}) %all-to-all-start) | async-done | bytes 1048608 | tf_op jit(solution)/shard_map/all_to_all | solution.py:23
  40.7 10.6 %all-to-all-start.4 = ((bf16[32,32,256]{2,1,0:T(8,128)(2,1)}), bf16[32,32,256]{2,1,0:T(8,128)(2,1)S(1)}, u32[]{:S(2)}, u32[]{:S(2)}) async-start(bf16[32,32,256]{2,1,0:T(8,128)(2,1)} %broadcast_in_dim.8), calls=%async_computation.4 | async-start | bytes 1048576 | tf_op jit(solution)/shard_map/all_to_all | solution.py:23
  54.7 14.1 %all-to-all-done.4 = bf16[32,32,256]{2,1,0:T(8,128)(2,1)S(1)} async-done(((bf16[32,32,256]{2,1,0:T(8,128)(2,1)}), bf16[32,32,256]{2,1,0:T(8,128)(2,1)S(1)}, u32[]{:S(2)}, u32[]{:S(2)}) %all-to-all-start.4) | async-done | bytes 524320 | tf_op jit(solution)/shard_map/all_to_all | solution.py:23
  68.8 4.7 %all-to-all-start.1 = ((bf16[32,4,2048]{2,1,0:T(4,128)(2,1)}), bf16[32,4,2048]{2,1,0:T(4,128)(2,1)S(1)}, u32[]{:S(2)}, u32[]{:S(2)}) async-start(bf16[32,4,2048]{2,1,0:T(4,128)(2,1)} %reshape.385), calls=%async_computation.1 | async-start | bytes 1048576 | tf_op jit(solution)/shard_map/all_to_all | solution.py:116
  73.5 1.2 convolution_convert_fusion.4
  74.7 2.0 convolution_convert_fusion.5
  76.7 1.2 copy.40
  77.9 1.4 reshape.391
  80.2 1.9 pad_maximum_fusion
  82.1 8.3 %all-to-all-done.1 = bf16[32,4,2048]{2,1,0:T(4,128)(2,1)S(1)} async-done(((bf16[32,4,2048]{2,1,0:T(4,128)(2,1)}), bf16[32,4,2048]{2,1,0:T(4,128)(2,1)S(1)}, u32[]{:S(2)}, u32[]{:S(2)}) %all-to-all-start.1) | async-done | bytes 524320 | tf_op jit(solution)/shard_map/all_to_all | solution.py:116
  90.6 2.0 fusion.3
  92.6 2.5 %convolution_convert_fusion = bf16[128,2048]{1,0:T(8,128)(2,1)S(1)} fusion(bf16[1,512,2048]{2,1,0:T(8,128)(2,1)S(1)} %copy-done, bf16[128,2048]{1,0:T(8,128)(2,1)S(1)} %reshape.386, bf16[1,2048,512]{2,1,0:T(8,128)(2,1)} %param.38, f32[128,512]{1,0:T(8,128)S(1)} %fusion.3), kind=kOutput, calls=%fused_computation.1 | convolution fusion | flops 537526272 | bytes 5505024 | tf_op jit(solution)/shard_map/dot_general | solution.py:122
  95.9 6.1 %all-to-all-start.2 = ((bf16[8,128,256]{2,1,0:T(8,128)(2,1)}), bf16[8,128,256]{2,1,0:T(8,128)(2,1)}, u32[]{:S(2)}, u32[]{:S(2)}) async-start(bf16[8,128,256]{2,1,0:T(8,128)(2,1)} %bitcast.85), calls=%async_computation.2 | async-start | bytes 1048576 | tf_op jit(solution)/shard_map/all_to_all | solution.py:17
  102.0 47.7 %all-reduce.2.cloned.1.call-done = bf16[360448]{0:T(1024)(128)(2,1)} async-done(((bf16[360448]{0:T(1024)(128)(2,1)}), bf16[360448]{0:T(1024)(128)(2,1)}) %all-reduce.2.cloned.1.call-update) | async-done | bytes 720912 | tf_op jit(solution)/shard_map/psum | solution.py:44
  149.8 1.2 slice_convert_fusion.1
  150.9 1.7 reshape.401
  152.7 1.7 reshape.402
  154.4 1.1 reduce_sum.102
  156.1 9.8 %all-to-all-start.3 = ((bf16[32,4,256]{2,1,0:T(4,128)(2,1)}), bf16[32,4,256]{2,1,0:T(4,128)(2,1)S(1)}, u32[]{:S(2)}, u32[]{:S(2)}) async-start(bf16[32,4,256]{2,1,0:T(4,128)(2,1)} %reshape.388), calls=%async_computation.3 | async-start | bytes 131072 | tf_op jit(solution)/shard_map/all_to_all | solution.py:124
  166.0 2.8 %convolution_convert_fusion.3 = bf16[1024,256]{1,0:T(8,128)(2,1)} fusion(bf16[176,256]{1,0:T(8,128)(2,1)S(1)} %copy-done.17, f32[1024,176]{1,0:T(8,128)} %reshape.402, f32[1024,176]{1,0:T(8,128)} %reshape.401), kind=kOutput, calls=%fused_computation.13 | convolution fusion | flops 93618176 | bytes 2056192 | tf_op jit(solution)/shard_map/dot_general | solution.py:210
  168.8 7.4 %all-to-all-done.3 = bf16[32,4,256]{2,1,0:T(4,128)(2,1)S(1)} async-done(((bf16[32,4,256]{2,1,0:T(4,128)(2,1)}), bf16[32,4,256]{2,1,0:T(4,128)(2,1)S(1)}, u32[]{:S(2)}, u32[]{:S(2)}) %all-to-all-start.3) | async-done | bytes 65568 | tf_op jit(solution)/shard_map/all_to_all | solution.py:124
  176.2 3.9 %all-to-all-start.5 = ((bf16[32,32,256]{2,1,0:T(8,128)(2,1)}), bf16[32,32,256]{2,1,0:T(8,128)(2,1)S(1)}, u32[]{:S(2)}, u32[]{:S(2)}) async-start(bf16[32,32,256]{2,1,0:T(8,128)(2,1)} %bitcast.18), calls=%async_computation.5 | async-start | bytes 1048576 | tf_op jit(solution)/shard_map/all_to_all | solution.py:17
  180.4 2.9 %multiply_add_fusion = f32[32,1,128,128]{3,2,1,0:T(8,128)} fusion(f32[32,1,128,128]{3,2,1,0:T(8,128)} %param.28, f32[32,128]{1,0:T(8,128)S(1)} %copy-done.9, f32[32,128]{1,0:T(8,128)S(1)} %maximum_multiply_fusion.1, f32[]{:T(128)S(6)} %sub.37), kind=kLoop, calls=%fused_computation.11 | loop fusion | flops 1572864 | bytes 4227076 | tf_op jit(solution)/shard_map/add | solution.py:83
  184.4 13.4 %all-to-all-done.5 = bf16[32,32,256]{2,1,0:T(8,128)(2,1)S(1)} async-done(((bf16[32,32,256]{2,1,0:T(8,128)(2,1)}), bf16[32,32,256]{2,1,0:T(8,128)(2,1)S(1)}, u32[]{:S(2)}, u32[]{:S(2)}) %all-to-all-start.5) | async-done | bytes 524320 | tf_op jit(solution)/shard_map/all_to_all | solution.py:17
  197.9 1.4 add_convert_fusion
  (86 shorter events, 13.0 us)
Async XLA Ops:
  7.2 85.5 %copy-start = (bf16[1,512,2048]{2,1,0:T(8,128)(2,1)S(1)}, bf16[1,512,2048]{2,1,0:T(8,128)(2,1)}, u32[]{:S(2)}) copy-start(bf16[1,512,2048]{2,1,0:T(8,128)(2,1)} %param.39) | copy-start | bytes 6291460
  7.2 8.4 %copy-start.1 = (bf16[32,2048]{1,0:T(8,128)(2,1)S(1)}, bf16[32,2048]{1,0:T(8,128)(2,1)}, u32[]{:S(2)}) copy-start(bf16[32,2048]{1,0:T(8,128)(2,1)} %param.20) | copy-start | bytes 393220
  7.2 8.4 %copy-start.5 = (bf16[2048,128]{1,0:T(8,128)(2,1)S(1)}, bf16[2048,128]{1,0:T(8,128)(2,1)}, u32[]{:S(2)}) copy-start(bf16[2048,128]{1,0:T(8,128)(2,1)} %param.24) | copy-start | bytes 1572868
  10.5 6.3 %copy-start.6 = (bf16[128,2048]{1,0:T(8,128)(2,1)S(1)}, bf16[128,2048]{1,0:T(8,128)(2,1)}, u32[]{:S(2)}) copy-start(bf16[128,2048]{1,0:T(8,128)(2,1)} %param.27) | copy-start | bytes 1572868
  13.4 4.9 %copy-start.7 = (f32[32,1,64]{2,0,1:T(8,128)}, f32[32,1,64]{2,0,1:T(8,128)S(1)}, u32[]{:S(2)}) copy-start(f32[32,1,64]{2,0,1:T(8,128)S(1)} %get-tuple-element.15) | copy-start | bytes 24580
  16.8 8.1 %copy-start.10 = (bf16[2048]{0:T(1024)(128)(2,1)S(1)}, bf16[2048]{0:T(1024)(128)(2,1)}, u32[]{:S(2)}) copy-start(bf16[2048]{0:T(1024)(128)(2,1)} %param.30) | copy-start | bytes 12292
  16.8 8.1 %copy-start.12 = (s32[32,2]{0,1:T(2,128)S(1)}, s32[32,2]{0,1:T(2,128)}, u32[]{:S(2)}) copy-start(s32[32,2]{0,1:T(2,128)} %param.35) | copy-start | bytes 772
  19.5 19.3 %all-to-all-start = ((bf16[8,32,2048]{2,1,0:T(8,128)(2,1)}), bf16[8,32,2048]{2,1,0:T(8,128)(2,1)S(1)}, u32[]{:S(2)}, u32[]{:S(2)}) async-start(bf16[8,32,2048]{2,1,0:T(8,128)(2,1)} %broadcast_in_dim.6), calls=%async_computation | async-start | bytes 2097152 | tf_op jit(solution)/shard_map/all_to_all | solution.py:23
  39.0 0.7 copy-start.2
  39.9 13.4 %copy-start.3 = (bf16[32,2048]{1,0:T(8,128)(2,1)}, bf16[32,2048]{1,0:T(8,128)(2,1)S(1)}, u32[]{:S(2)}) copy-start(bf16[32,2048]{1,0:T(8,128)(2,1)S(1)} %multiply_convert_fusion.2) | copy-start | bytes 393220
  40.7 28.1 %all-to-all-start.4 = ((bf16[32,32,256]{2,1,0:T(8,128)(2,1)}), bf16[32,32,256]{2,1,0:T(8,128)(2,1)S(1)}, u32[]{:S(2)}, u32[]{:S(2)}) async-start(bf16[32,32,256]{2,1,0:T(8,128)(2,1)} %broadcast_in_dim.8), calls=%async_computation.4 | async-start | bytes 1048576 | tf_op jit(solution)/shard_map/all_to_all | solution.py:23
  52.6 0.5 copy-start.13
  68.8 21.7 %all-to-all-start.1 = ((bf16[32,4,2048]{2,1,0:T(4,128)(2,1)}), bf16[32,4,2048]{2,1,0:T(4,128)(2,1)S(1)}, u32[]{:S(2)}, u32[]{:S(2)}) async-start(bf16[32,4,2048]{2,1,0:T(4,128)(2,1)} %reshape.385), calls=%async_computation.1 | async-start | bytes 1048576 | tf_op jit(solution)/shard_map/all_to_all | solution.py:116
  73.5 76.3 %all-reduce.2.cloned.1.call-start = ((), (), s32[]{:S(2)}) async-start(), calls=%async_computation.6 | async-start | bytes 1441792 | tf_op jit(solution)/shard_map/psum | solution.py:44
  95.9 58.4 %all-to-all-start.2 = ((bf16[8,128,256]{2,1,0:T(8,128)(2,1)}), bf16[8,128,256]{2,1,0:T(8,128)(2,1)}, u32[]{:S(2)}, u32[]{:S(2)}) async-start(bf16[8,128,256]{2,1,0:T(8,128)(2,1)} %bitcast.85), calls=%async_computation.2 | async-start | bytes 1048576 | tf_op jit(solution)/shard_map/all_to_all | solution.py:17
  152.7 13.3 %copy-start.17 = (bf16[176,256]{1,0:T(8,128)(2,1)S(1)}, bf16[176,256]{1,0:T(8,128)(2,1)}, u32[]{:S(2)}) copy-start(bf16[176,256]{1,0:T(8,128)(2,1)} %param.34) | copy-start | bytes 270340
  156.1 20.1 %all-to-all-start.3 = ((bf16[32,4,256]{2,1,0:T(4,128)(2,1)}), bf16[32,4,256]{2,1,0:T(4,128)(2,1)S(1)}, u32[]{:S(2)}, u32[]{:S(2)}) async-start(bf16[32,4,256]{2,1,0:T(4,128)(2,1)} %reshape.388), calls=%async_computation.3 | async-start | bytes 131072 | tf_op jit(solution)/shard_map/all_to_all | solution.py:124
  166.0 14.1 %copy-start.14 = (s32[64]{0:T(128)S(1)}, s32[64]{0:T(128)}, u32[]{:S(2)}) copy-start(s32[64]{0:T(128)} %copy-done.13) | copy-start | bytes 772
  166.0 14.1 %copy-start.16 = (s32[64,1]{0,1:T(1,128)S(1)}, s32[64,1]{0,1:T(1,128)}, u32[]{:S(2)}) copy-start(s32[64,1]{0,1:T(1,128)} %mul.310) | copy-start | bytes 772
  166.0 14.1 %copy-start.11 = (bf16[2048]{0:T(1024)(128)(2,1)S(1)}, bf16[2048]{0:T(1024)(128)(2,1)}, u32[]{:S(2)}) copy-start(bf16[2048]{0:T(1024)(128)(2,1)} %param.31) | copy-start | bytes 12292
  166.0 14.2 %copy-start.15 = (bf16[32,2]{0,1:T(2,128)(2,1)S(1)}, bf16[32,2]{0,1:T(2,128)(2,1)}, u32[]{:S(2)}) copy-start(bf16[32,2]{0,1:T(2,128)(2,1)} %param.36) | copy-start | bytes 388
  166.0 14.3 %copy-start.8 = (f32[32,1,64]{2,0,1:T(8,128)S(1)}, f32[32,1,64]{2,0,1:T(8,128)}, u32[]{:S(2)}) copy-start(f32[32,1,64]{2,0,1:T(8,128)} %copy-done.7) | copy-start | bytes 24580
  166.0 14.3 %copy-start.9 = (f32[32,128]{1,0:T(8,128)S(1)}, f32[32,128]{1,0:T(8,128)}, u32[]{:S(2)}) copy-start(f32[32,128]{1,0:T(8,128)} %get-tuple-element.16) | copy-start | bytes 49156
  176.2 21.6 %all-to-all-start.5 = ((bf16[32,32,256]{2,1,0:T(8,128)(2,1)}), bf16[32,32,256]{2,1,0:T(8,128)(2,1)S(1)}, u32[]{:S(2)}, u32[]{:S(2)}) async-start(bf16[32,32,256]{2,1,0:T(8,128)(2,1)} %bitcast.18), calls=%async_computation.5 | async-start | bytes 1048576 | tf_op jit(solution)/shard_map/all_to_all | solution.py:17
  180.4 2.9 %copy-start.4 = (bf16[32,2048]{1,0:T(8,128)(2,1)S(1)}, bf16[32,2048]{1,0:T(8,128)(2,1)}, u32[]{:S(2)}) copy-start(bf16[32,2048]{1,0:T(8,128)(2,1)} %copy-done.3) | copy-start | bytes 393220
Sparse Core Ops, SparseCore 0:
  82.2 67.4 all-reduce.1
where the time goes:
time: 207 us; the launch traced here: 206 us
  waiting for transfers between devices  105 us (51%)
  starting transfers between devices  40.5 us (20%)
  matrix products  18.1 us (9%)
  local copies, waits for them, and re-layouts  14.9 us (7%)
  between operations  14.5 us (7%)
  other arithmetic  13.4 us (6%)
    psum x1, waiting for transfers between devices, packed_total(): running = lax.psum(flat, axis)  47.7 us
    all_to_all x2, waiting for transfers between devices, copy_for_each(): return lax.all_to_all(copies, axis, split_axis=0, concat_axis=0, tiled=True)  27.9 us
    all_to_all x2, starting transfers between devices, copy_for_each(): return lax.all_to_all(copies, axis, split_axis=0, concat_axis=0, tiled=True)  16 us
    all_to_all x2, waiting for transfers between devices, sent_and_summed(): lax.all_to_all(tiles, axis, split_axis=0, concat_axis=0, tiled=True)  13.4 us
    all_to_all x2, starting transfers between devices, sent_and_summed(): lax.all_to_all(tiles, axis, split_axis=0, concat_axis=0, tiled=True)  9.98 us
    all_to_all x1, starting transfers between devices, padded_experts(): lax.all_to_all(summed.reshape(sources, items, summed.shape[1]), 'ep', spl...  9.82 us
    all_to_all x1, waiting for transfers between devices, padded_experts(): lax.all_to_all(outgoing, 'ep', split_axis=0, concat_axis=0, tiled=True)  8.34 us
    all_to_all x1, waiting for transfers between devices, padded_experts(): lax.all_to_all(summed.reshape(sources, items, summed.shape[1]), 'ep', spl...  7.39 us
  transfers between devices with their start and end apart: 7, of which 6 were waited for; matrix products, arithmetic and copies ran while one was open for 14% of the time, Pallas kernels for 0%

commit v1 on v0

--- a/solution.py
+++ b/solution.py
@@ -7,6 +7,10 @@
 THETA = 10000.0
 
 
+def zones_number(axis_key, here_x):
+    return jnp.sum(lax.all_gather(here_x, axis_name=axis_key), 0)
+
+
 def split_up(value, dim, length):
     before, after = (value.shape[:dim], value.shape[dim + 1 :])
     return jnp.moveaxis(value.reshape(*before, length, -1, *after), dim, 0)
@@ -41,7 +45,7 @@
 
 def packed_total(arrays, axis):
     flat, at, outs = (jnp.concatenate([a.reshape(-1) for a in arrays]), 0, [])
-    running = lax.psum(flat, axis)
+    running = zones_number(axis, flat)
     for a in arrays:
         outs.append(running[at : at + a.size].reshape(a.shape))
         at += a.size

time: 207 us -> 191 us (0.923)
  waiting for transfers between devices: 105 us -> 33.6 us
  blocking collectives: 0 us -> 49.4 us
  starting transfers between devices: 40.5 us -> 27.6 us
  other arithmetic: 13.4 us -> 25.4 us
  local copies, waits for them, and re-layouts: 14.9 us -> 21.6 us
    all_to_all x0 -> x2, blocking collectives: none -> 49.4 us  [the longest x1 27.9 us: copy_for_each(): return lax.all_to_all(copies, axis, split_axis=0, concat_axis=0, tiled=True)]
    psum x1 -> x0, waiting for transfers between devices: 47.7 us -> none  [packed_total(): running = lax.psum(flat, axis)]
    reduce_sum x0 -> x1, other arithmetic: none -> 14.3 us  [zones_number(): return jnp.sum(lax.all_gather(here_x, axis_name=axis_key), 0)]
    all_to_all x2 -> x1, waiting for transfers between devices: 27.9 us -> 13.8 us  [copy_for_each(): return lax.all_to_all(copies, axis, split_axis=0, concat_axis=0, tiled=True)]
    all_to_all x2 -> x1, starting transfers between devices: 16 us -> 5.42 us  [copy_for_each(): return lax.all_to_all(copies, axis, split_axis=0, concat_axis=0, tiled=True)]
    all_to_all x1 -> x0, waiting for transfers between devices: 8.34 us -> none  [padded_experts(): lax.all_to_all(outgoing, 'ep', split_axis=0, concat_axis=0, tiled=True)]
    all_gather x0 -> x1, local copies, waits for them, and re-layouts: none -> 7.62 us  [zones_number(): return jnp.sum(lax.all_gather(here_x, axis_name=axis_key), 0)]
    all_to_all x1, waiting for transfers between devices: 7.39 us -> 0.01 us  [padded_experts(): lax.all_to_all(summed.reshape(sources, items, summed.shape[1]), 'ep', spl...]
  transfers between devices with their start and end apart: 7 -> 5, of which waited for: 6 -> 3; matrix products, arithmetic and copies ran while one was open for 14% -> 24% of each run, Pallas kernels for 0% -> 0%
where the time goes in v1:
time: 191 us; the launch traced here: 189 us
  blocking collectives  49.4 us (26%)
  waiting for transfers between devices  33.6 us (18%)
  starting transfers between devices  27.6 us (14%)
  other arithmetic  25.4 us (13%)
  local copies, waits for them, and re-layouts  21.6 us (11%)
  matrix products  16.5 us (9%)
  between operations  14.5 us (8%)
    all_to_all x1, blocking collectives, copy_for_each(): return lax.all_to_all(copies, axis, split_axis=0, concat_axis=0, tiled=True)  27.9 us
    all_to_all x1, blocking collectives, padded_experts(): lax.all_to_all(outgoing, 'ep', split_axis=0, concat_axis=0, tiled=True)  21.5 us
    all_to_all x2, waiting for transfers between devices, sent_and_summed(): lax.all_to_all(tiles, axis, split_axis=0, concat_axis=0, tiled=True)  19.7 us
    all_to_all x2, starting transfers between devices, sent_and_summed(): lax.all_to_all(tiles, axis, split_axis=0, concat_axis=0, tiled=True)  15 us
    reduce_sum x1, other arithmetic, zones_number(): return jnp.sum(lax.all_gather(here_x, axis_name=axis_key), 0)  14.3 us
    all_to_all x1, waiting for transfers between devices, copy_for_each(): return lax.all_to_all(copies, axis, split_axis=0, concat_axis=0, tiled=True)  13.8 us
    all_gather x1, local copies, waits for them, and re-layouts, zones_number(): return jnp.sum(lax.all_gather(here_x, axis_name=axis_key), 0)  7.62 us
    all_to_all x1, starting transfers between devices, padded_experts(): lax.all_to_all(summed.reshape(sources, items, summed.shape[1]), 'ep', spl...  7.24 us
  transfers between devices with their start and end apart: 5, of which 3 were waited for; matrix products, arithmetic and copies ran while one was open for 24% of the time, Pallas kernels for 0%

profile of v1, /device:TPU:24, one launch (start us, length us, event | category | flops | bytes accessed | tf_op | source)
XLA Modules:
  0.0 188.7 jit_solution(4754616117765025900)
XLA Ops:
  7.3 0.8 convert_element_type.128
  8.7 1.0 fusion.25
  10.5 1.4 fusion.18
  11.9 1.4 fusion.20
  13.6 2.0 %fusion.66 = f32[32,1,128]{2,1,0:T(1,128)S(1)} fusion(f32[32,128,1]{1,2,0:T(1,128)S(1)} %bitcast.92, f32[32,1,128,128]{3,2,1,0:T(8,128)} %param.28), kind=kOutput, calls=%fused_computation.103 | convolution fusion | flops 1048576 | bytes 2129920 | tf_op jit(solution)/shard_map/shd,shde->she/dot_general | solution.py:84
  15.6 1.0 fusion.65
  16.8 1.5 convolution_convert_fusion.2
  18.4 1.1 broadcast_in_dim.6
  19.5 5.4 %all-to-all-start = ((bf16[8,32,2048]{2,1,0:T(8,128)(2,1)}), bf16[8,32,2048]{2,1,0:T(8,128)(2,1)S(1)}, u32[]{:S(2)}, u32[]{:S(2)}) async-start(bf16[8,32,2048]{2,1,0:T(8,128)(2,1)} %broadcast_in_dim.6), calls=%async_computation | async-start | bytes 2097152 | tf_op jit(solution)/shard_map/all_to_all | solution.py:27
  24.9 13.8 %all-to-all-done = bf16[8,32,2048]{2,1,0:T(8,128)(2,1)S(1)} async-done(((bf16[8,32,2048]{2,1,0:T(8,128)(2,1)}), bf16[8,32,2048]{2,1,0:T(8,128)(2,1)S(1)}, u32[]{:S(2)}, u32[]{:S(2)}) %all-to-all-start) | async-done | bytes 1048608 | tf_op jit(solution)/shard_map/all_to_all | solution.py:27
  39.8 27.9 %all_to_all.30 = bf16[32,32,256]{2,1,0:T(8,128)(2,1)S(1)} all-to-all(bf16[32,32,256]{2,1,0:T(8,128)(2,1)S(1)} %broadcast_in_dim.8), channel_id=1, replica_groups=mesh['ep'=32,'tp'=8] {'ep'}, dimensions={0} | all-to-all | bytes 1048576 | tf_op jit(solution)/shard_map/all_to_all | solution.py:27
  67.6 1.2 convolution_convert_fusion.4
  71.0 0.9 pad_maximum_fusion
  73.3 21.5 %all_to_all.31 = bf16[32,4,2048]{2,1,0:T(4,128)(2,1)} all-to-all(bf16[32,4,2048]{2,1,0:T(4,128)(2,1)S(1)} %reshape.385), channel_id=1, replica_groups=mesh['ep'=32,'tp'=8] {'ep'}, dimensions={0} | all-to-all | bytes 1048576 | tf_op jit(solution)/shard_map/all_to_all | solution.py:120
  94.9 1.2 reshape.386
  96.0 2.0 %fusion.3 = f32[128,512]{1,0:T(8,128)S(1)} fusion(bf16[128,2048]{1,0:T(8,128)(2,1)S(1)} %reshape.386, bf16[1,2048,512]{2,1,0:T(8,128)(2,1)} %param.37), kind=kOutput, calls=%fused_computation.7 | convolution fusion | flops 268435456 | bytes 2883584 | tf_op jit(solution)/shard_map/dot_general | solution.py:100
  98.1 2.5 %convolution_convert_fusion = bf16[128,2048]{1,0:T(8,128)(2,1)S(1)} fusion(bf16[1,512,2048]{2,1,0:T(8,128)(2,1)S(1)} %copy-done, bf16[128,2048]{1,0:T(8,128)(2,1)S(1)} %reshape.386, bf16[1,2048,512]{2,1,0:T(8,128)(2,1)} %param.38, f32[128,512]{1,0:T(8,128)S(1)} %fusion.3), kind=kOutput, calls=%fused_computation.1 | convolution fusion | flops 537526272 | bytes 5505024 | tf_op jit(solution)/shard_map/dot_general | solution.py:126
  100.6 0.8 copy.46
  101.4 5.5 %all-to-all-start.2 = ((bf16[8,128,256]{2,1,0:T(8,128)(2,1)}), bf16[8,128,256]{2,1,0:T(8,128)(2,1)S(1)}, u32[]{:S(2)}, u32[]{:S(2)}) async-start(bf16[8,128,256]{2,1,0:T(8,128)(2,1)} %bitcast.85), calls=%async_computation.2 | async-start | bytes 1048576 | tf_op jit(solution)/shard_map/all_to_all | solution.py:21
  107.6 7.5 %all-to-all-done.2 = bf16[8,128,256]{2,1,0:T(8,128)(2,1)S(1)} async-done(((bf16[8,128,256]{2,1,0:T(8,128)(2,1)}), bf16[8,128,256]{2,1,0:T(8,128)(2,1)S(1)}, u32[]{:S(2)}, u32[]{:S(2)}) %all-to-all-start.2) | async-done | bytes 524320 | tf_op jit(solution)/shard_map/all_to_all | solution.py:21
  115.8 7.2 %all-to-all-start.3 = ((bf16[32,4,256]{2,1,0:T(4,128)(2,1)}), bf16[32,4,256]{2,1,0:T(4,128)(2,1)}, u32[]{:S(2)}, u32[]{:S(2)}) async-start(bf16[32,4,256]{2,1,0:T(4,128)(2,1)} %reshape.388), calls=%async_computation.3 | async-start | bytes 131072 | tf_op jit(solution)/shard_map/all_to_all | solution.py:128
  123.1 7.6 %reshape.412 = bf16[8,360448]{1,0:T(8,128)(2,1)} reshape(bf16[2883584]{0:T(1024)(128)(2,1)} %all-gather.3.cloned.1.call-done) | data formatting | bytes 11534336 | tf_op jit(solution)/shard_map/all_gather | solution.py:11
  130.7 14.3 %reduce_sum.117 = bf16[360448]{0:T(1024)(128)(2,1)S(1)} reduce(bf16[8,360448]{1,0:T(8,128)(2,1)} %reshape.412, bf16[]{:T(256)} %constant.62.clone.1), dimensions={0}, to_apply=%region_10.11 | reduce | flops 2523136 | bytes 6488066 | tf_op jit(solution)/shard_map/reduce_sum | solution.py:11
  145.0 1.0 slice_convert_fusion.1
  146.0 2.9 %reshape.401 = f32[1024,176]{1,0:T(8,128)} reshape(f32[180224]{0:T(1024)} %get-tuple-element.8) | data formatting | bytes 1441792 | tf_op jit(solution)/shard_map/convert_element_type | solution.py:206
  148.9 1.7 reshape.402
  150.6 2.8 %convolution_convert_fusion.3 = bf16[1024,256]{1,0:T(8,128)(2,1)} fusion(bf16[176,256]{1,0:T(8,128)(2,1)S(1)} %copy-done.19, f32[1024,176]{1,0:T(8,128)} %reshape.402, f32[1024,176]{1,0:T(8,128)} %reshape.401), kind=kOutput, calls=%fused_computation.13 | convolution fusion | flops 93618176 | bytes 2056192 | tf_op jit(solution)/shard_map/dot_general | solution.py:214
  153.4 9.5 %all-to-all-start.5 = ((bf16[32,32,256]{2,1,0:T(8,128)(2,1)}), bf16[32,32,256]{2,1,0:T(8,128)(2,1)S(1)}, u32[]{:S(2)}, u32[]{:S(2)}) async-start(bf16[32,32,256]{2,1,0:T(8,128)(2,1)} %bitcast.18), calls=%async_computation.5 | async-start | bytes 1048576 | tf_op jit(solution)/shard_map/all_to_all | solution.py:21
  163.2 2.9 %multiply_add_fusion = f32[32,1,128,128]{3,2,1,0:T(8,128)} fusion(f32[32,1,128,128]{3,2,1,0:T(8,128)} %param.28, f32[32,128]{1,0:T(8,128)S(1)} %copy-done.10, f32[32,128]{1,0:T(8,128)S(1)} %maximum_multiply_fusion.1, f32[]{:T(128)S(6)} %sub.37), kind=kLoop, calls=%fused_computation.11 | loop fusion | flops 1572864 | bytes 4227076 | tf_op jit(solution)/shard_map/add | solution.py:87
  166.3 0.9 reshape.389
  168.1 12.2 %all-to-all-done.5 = bf16[32,32,256]{2,1,0:T(8,128)(2,1)S(1)} async-done(((bf16[32,32,256]{2,1,0:T(8,128)(2,1)}), bf16[32,32,256]{2,1,0:T(8,128)(2,1)S(1)}, u32[]{:S(2)}, u32[]{:S(2)}) %all-to-all-start.5) | async-done | bytes 524320 | tf_op jit(solution)/shard_map/all_to_all | solution.py:21
  180.4 1.4 add_convert_fusion
  (90 shorter events, 9.2 us)
Async XLA Ops:
  7.2 90.9 %copy-start = (bf16[1,512,2048]{2,1,0:T(8,128)(2,1)S(1)}, bf16[1,512,2048]{2,1,0:T(8,128)(2,1)}, u32[]{:S(2)}) copy-start(bf16[1,512,2048]{2,1,0:T(8,128)(2,1)} %param.39) | copy-start | bytes 6291460
  7.2 8.4 %copy-start.1 = (bf16[32,2048]{1,0:T(8,128)(2,1)S(1)}, bf16[32,2048]{1,0:T(8,128)(2,1)}, u32[]{:S(2)}) copy-start(bf16[32,2048]{1,0:T(8,128)(2,1)} %param.20) | copy-start | bytes 393220
  7.2 8.4 %copy-start.5 = (bf16[2048,128]{1,0:T(8,128)(2,1)S(1)}, bf16[2048,128]{1,0:T(8,128)(2,1)}, u32[]{:S(2)}) copy-start(bf16[2048,128]{1,0:T(8,128)(2,1)} %param.24) | copy-start | bytes 1572868
  10.5 6.3 %copy-start.6 = (bf16[128,2048]{1,0:T(8,128)(2,1)S(1)}, bf16[128,2048]{1,0:T(8,128)(2,1)}, u32[]{:S(2)}) copy-start(bf16[128,2048]{1,0:T(8,128)(2,1)} %param.27) | copy-start | bytes 1572868
  13.4 4.9 %copy-start.7 = (f32[32,1,64]{2,0,1:T(8,128)}, f32[32,1,64]{2,0,1:T(8,128)S(1)}, u32[]{:S(2)}) copy-start(f32[32,1,64]{2,0,1:T(8,128)S(1)} %get-tuple-element.15) | copy-start | bytes 24580
  16.8 8.1 %copy-start.11 = (bf16[2048]{0:T(1024)(128)(2,1)S(1)}, bf16[2048]{0:T(1024)(128)(2,1)}, u32[]{:S(2)}) copy-start(bf16[2048]{0:T(1024)(128)(2,1)} %param.30) | copy-start | bytes 12292
  19.5 19.3 %all-to-all-start = ((bf16[8,32,2048]{2,1,0:T(8,128)(2,1)}), bf16[8,32,2048]{2,1,0:T(8,128)(2,1)S(1)}, u32[]{:S(2)}, u32[]{:S(2)}) async-start(bf16[8,32,2048]{2,1,0:T(8,128)(2,1)} %broadcast_in_dim.6), calls=%async_computation | async-start | bytes 2097152 | tf_op jit(solution)/shard_map/all_to_all | solution.py:27
  24.9 98.2 %all-gather.3.cloned.1.call-start = ((), (), s32[]{:S(2)}) async-start(), calls=%async_computation.6 | async-start | bytes 6488064 | tf_op jit(solution)/shard_map/all_gather | solution.py:11
  38.9 30.0 %copy-start.9 = (bf16[256,176]{0,1:T(8,128)(2,1)S(1)}, bf16[256,176]{0,1:T(8,128)(2,1)}, u32[]{:S(2)}) copy-start(bf16[256,176]{0,1:T(8,128)(2,1)} %param.32) | copy-start | bytes 270340
  39.0 0.7 copy-start.2
  39.1 33.4 %copy-start.3 = (bf16[32,2048]{1,0:T(8,128)(2,1)}, bf16[32,2048]{1,0:T(8,128)(2,1)S(1)}, u32[]{:S(2)}) copy-start(bf16[32,2048]{1,0:T(8,128)(2,1)S(1)} %multiply_convert_fusion.2) | copy-start | bytes 393220
  70.1 1.9 copy-start.13
  72.5 23.5 %copy-start.15 = (s32[64]{0:T(128)}, s32[64]{0:T(128)S(1)}, u32[]{:S(2)}) copy-start(s32[64]{0:T(128)S(1)} %select_reduce_fusion) | copy-start | bytes 772
  100.6 6.3 %copy-start.14 = (s32[32,2]{0,1:T(2,128)S(1)}, s32[32,2]{0,1:T(2,128)}, u32[]{:S(2)}) copy-start(s32[32,2]{0,1:T(2,128)} %param.35) | copy-start | bytes 772
  101.4 13.7 %all-to-all-start.2 = ((bf16[8,128,256]{2,1,0:T(8,128)(2,1)}), bf16[8,128,256]{2,1,0:T(8,128)(2,1)S(1)}, u32[]{:S(2)}, u32[]{:S(2)}) async-start(bf16[8,128,256]{2,1,0:T(8,128)(2,1)} %bitcast.85), calls=%async_computation.2 | async-start | bytes 1048576 | tf_op jit(solution)/shard_map/all_to_all | solution.py:21
  115.8 37.6 %all-to-all-start.3 = ((bf16[32,4,256]{2,1,0:T(4,128)(2,1)}), bf16[32,4,256]{2,1,0:T(4,128)(2,1)}, u32[]{:S(2)}, u32[]{:S(2)}) async-start(bf16[32,4,256]{2,1,0:T(4,128)(2,1)} %reshape.388), calls=%async_computation.3 | async-start | bytes 131072 | tf_op jit(solution)/shard_map/all_to_all | solution.py:128
  146.0 4.6 %copy-start.19 = (bf16[176,256]{1,0:T(8,128)(2,1)S(1)}, bf16[176,256]{1,0:T(8,128)(2,1)}, u32[]{:S(2)}) copy-start(bf16[176,256]{1,0:T(8,128)(2,1)} %param.34) | copy-start | bytes 270340
  150.6 12.4 %copy-start.16 = (s32[64]{0:T(128)S(1)}, s32[64]{0:T(128)}, u32[]{:S(2)}) copy-start(s32[64]{0:T(128)} %copy-done.15) | copy-start | bytes 772
  150.6 12.4 %copy-start.18 = (s32[64,1]{0,1:T(1,128)S(1)}, s32[64,1]{0,1:T(1,128)}, u32[]{:S(2)}) copy-start(s32[64,1]{0,1:T(1,128)} %mul.310) | copy-start | bytes 772
  150.6 12.4 %copy-start.12 = (bf16[2048]{0:T(1024)(128)(2,1)S(1)}, bf16[2048]{0:T(1024)(128)(2,1)}, u32[]{:S(2)}) copy-start(bf16[2048]{0:T(1024)(128)(2,1)} %param.31) | copy-start | bytes 12292
  150.6 12.4 %copy-start.17 = (bf16[32,2]{0,1:T(2,128)(2,1)S(1)}, bf16[32,2]{0,1:T(2,128)(2,1)}, u32[]{:S(2)}) copy-start(bf16[32,2]{0,1:T(2,128)(2,1)} %param.36) | copy-start | bytes 388
  150.6 12.5 %copy-start.8 = (f32[32,1,64]{2,0,1:T(8,128)S(1)}, f32[32,1,64]{2,0,1:T(8,128)}, u32[]{:S(2)}) copy-start(f32[32,1,64]{2,0,1:T(8,128)} %copy-done.7) | copy-start | bytes 24580
  150.6 12.6 %copy-start.10 = (f32[32,128]{1,0:T(8,128)S(1)}, f32[32,128]{1,0:T(8,128)}, u32[]{:S(2)}) copy-start(f32[32,128]{1,0:T(8,128)} %get-tuple-element.16) | copy-start | bytes 49156
  153.4 26.9 %all-to-all-start.5 = ((bf16[32,32,256]{2,1,0:T(8,128)(2,1)}), bf16[32,32,256]{2,1,0:T(8,128)(2,1)S(1)}, u32[]{:S(2)}, u32[]{:S(2)}) async-start(bf16[32,32,256]{2,1,0:T(8,128)(2,1)} %bitcast.18), calls=%async_computation.5 | async-start | bytes 1048576 | tf_op jit(solution)/shard_map/all_to_all | solution.py:21
  163.2 2.9 %copy-start.4 = (bf16[32,2048]{1,0:T(8,128)(2,1)S(1)}, bf16[32,2048]{1,0:T(8,128)(2,1)}, u32[]{:S(2)}) copy-start(bf16[32,2048]{1,0:T(8,128)(2,1)} %copy-done.3) | copy-start | bytes 393220
Sparse Core Ops, SparseCore 0:
  72.1 35.1 all-gather.2
